TPU v7x, 32 devices: a whole 2x2x4 slice. The times are simulated.
32 devices in a mesh: rep: 2 (over x), fs: 8 (over z, y), tp: 2 (over core).
Axes of the slice: x: 2, y: 2, z: 4, core: 2. Of those that a mesh axis runs over, the one named last changes fastest.
Arguments:
- incoming_features: bfloat16 [3072, 2048], P(('rep', 'fs'), 'tp'), may hold values from -6 to 6
- attend_prenormal_scale: bfloat16 [2048], replicated, may hold values from 0.099609375 to 1.8984375
- probe_matrix: bfloat16 [2048, 512], P('fs', 'tp'), may hold values from -0.125 to 0.125
- lookup_matrix: bfloat16 [2048, 512], P('fs', 'tp'), may hold values from -0.125 to 0.125
- content_matrix: bfloat16 [2048, 1024], P('fs', 'tp'), may hold values from -0.125 to 0.125
- forgetting_matrix: bfloat16 [2048, 512], P('fs', 'tp'), may hold values from -0.125 to 0.125
- result_switch_matrix: bfloat16 [2048, 1024], P('fs', 'tp'), may hold values from -0.125 to 0.125
- forgetting_shift: float32 [512], P('tp'), may hold values from -0.5 to 5.5
- spike_forget_logarithm: float32 [3072, 512], P(('rep', 'fs'), 'tp'), may hold values from -0.7 to 0
- attend_unit_scale: bfloat16 [1024], P('tp'), may hold values from 0.099609375 to 1.8984375
- attend_result_matrix: bfloat16 [1024, 2048], P('tp', 'fs'), may hold values from -0.1875 to 0.1875
- perceptron_scale: bfloat16 [2048], replicated, may hold values from 0.099609375 to 1.8984375
- content_expand_matrix: bfloat16 [2048, 4096], P('fs', 'tp'), may hold values from -0.125 to 0.125
- switch_expand_matrix: bfloat16 [2048, 4096], P('fs', 'tp'), may hold values from -0.125 to 0.125
- content_kernel: bfloat16 [3, 4096], P(None, 'tp'), may hold values from -3.5 to 3.5
- switch_kernel: bfloat16 [3, 4096], P(None, 'tp'), may hold values from -3.5 to 3.5
- contract_matrix: bfloat16 [4096, 2048], P('tp', 'fs'), may hold values from -0.09375 to 0.09375
Outputs:
- out_rows: bfloat16 [3072, 2048], P(('rep', 'fs'), 'tp')
All inputs are finite; a program needn't handle non-finite values.
Results may differ from a plain program's by a relative error of at most 0.02.
Values may be sent and summed in bfloat16 or wider, within the bound.
A program may use at most 64 MiB of HBM per device.

v0:
```python
import jax
import jax.numpy as jnp
from jax import lax
from jax.sharding import PartitionSpec as P

HEAD_K = 32
HEAD_V = 64
BLOCK = 64
norm_eps = 1e-06
switch_multiplier = 16.0


def row_norm(content_tokens, gain):
    content_tokens = content_tokens.astype(jnp.float32)
    scaled = content_tokens * lax.rsqrt(
        jnp.mean(content_tokens * content_tokens, axis=-1, keepdims=True) + norm_eps
    )
    return (scaled * gain.astype(jnp.float32)).astype(jnp.bfloat16)


def gated_scan(probe_tokens, lookup_tokens, content_tokens, forgetting_scores):
    length, heads, key_size = probe_tokens.shape
    value_size = content_tokens.shape[-1]
    blocks = length // BLOCK

    def split_blocks(array):
        return array.reshape(blocks, BLOCK, heads, array.shape[-1])

    causal = jnp.arange(BLOCK)[:, None] >= jnp.arange(BLOCK)[None, :]
    highest = lax.Precision.HIGHEST

    def step(state, incoming_tokens):
        query_block, key_block, value_block, decay_block = incoming_tokens
        cumulative = jnp.cumsum(decay_block, axis=0)
        differ = cumulative[:, None] - cumulative[None, :]
        weight = jnp.exp(jnp.where(causal[:, :, None, None], differ, -jnp.inf))
        scores = jnp.einsum("thd,shd,tshd->tsh", query_block, key_block, weight, precision=highest)
        inner = jnp.einsum("tsh,shv->thv", scores, value_block, precision=highest)
        carried = jnp.einsum(
            "thd,hdv->thv", query_block * jnp.exp(cumulative), state, precision=highest
        )
        final = cumulative[-1]
        state = jnp.exp(final)[:, :, None] * state + jnp.einsum(
            "shd,shv->hdv",
            key_block * jnp.exp(final[None] - cumulative),
            value_block,
            precision=highest,
        )
        return (state, inner + carried)

    start_state = jnp.zeros((heads, key_size, value_size), jnp.float32)
    _, result_tokens = lax.scan(
        step,
        start_state,
        (
            split_blocks(probe_tokens),
            split_blocks(lookup_tokens),
            split_blocks(content_tokens),
            split_blocks(forgetting_scores),
        ),
    )
    return result_tokens.reshape(length, heads, value_size)


def attend_unit_results(
    probe_tokens,
    lookup_tokens,
    content_tokens,
    result_switch,
    forgetting_raw,
    spike_forgetting,
    attend_unit_scale,
):
    length = probe_tokens.shape[0]
    heads = probe_tokens.shape[1] // HEAD_K
    forgetting_scores = jax.nn.log_sigmoid(forgetting_raw) / switch_multiplier + spike_forgetting

    def split_heads(array, width):
        return array.astype(jnp.float32).reshape(length, heads, width)

    result_tokens = gated_scan(
        split_heads(probe_tokens, HEAD_K) * HEAD_K ** (-0.5),
        split_heads(lookup_tokens, HEAD_K),
        split_heads(content_tokens, HEAD_V),
        split_heads(forgetting_scores, HEAD_K),
    )
    result_tokens = result_tokens * lax.rsqrt(
        jnp.mean(result_tokens * result_tokens, axis=-1, keepdims=True) + norm_eps
    )
    result_tokens = result_tokens * attend_unit_scale.astype(jnp.float32).reshape(heads, HEAD_V)
    switched_result = result_tokens.reshape(length, heads * HEAD_V) * jax.nn.silu(
        result_switch.astype(jnp.float32)
    )
    return switched_result.astype(jnp.bfloat16)


def causal_conv(content_tokens, taps):
    content_tokens = content_tokens.astype(jnp.float32)
    taps = taps.astype(jnp.float32)
    width = taps.shape[0]
    padded = jnp.pad(content_tokens, ((width - 1, 0), (0, 0)))
    total = jnp.zeros_like(content_tokens)
    for offset in range(width):
        total = total + padded[offset : offset + content_tokens.shape[0]] * taps[offset]
    return total


def shards(
    incoming_features,
    attend_prenormal_scale,
    probe_matrix,
    lookup_matrix,
    content_matrix,
    forgetting_matrix,
    result_switch_matrix,
    forgetting_shift,
    spike_forget_logarithm,
    attend_unit_scale,
    attend_result_matrix,
    perceptron_scale,
    content_expand_matrix,
    switch_expand_matrix,
    content_kernel,
    switch_kernel,
    contract_matrix,
):
    whole_in = lax.all_gather(incoming_features, "tp", axis=1, tiled=True)
    normed = row_norm(whole_in, attend_prenormal_scale)
    pieces = (
        lax.all_gather(probe_matrix, "fs", axis=0, tiled=True),
        lax.all_gather(lookup_matrix, "fs", axis=0, tiled=True),
        lax.all_gather(content_matrix, "fs", axis=0, tiled=True),
        lax.all_gather(forgetting_matrix, "fs", axis=0, tiled=True),
        lax.all_gather(result_switch_matrix, "fs", axis=0, tiled=True),
    )
    columns = normed
    query_sum, key_sum, value_sum, decay_sum, gate_sum = tuple(
        (jnp.dot(columns, piece, preferred_element_type=jnp.float32) for piece in pieces)
    )
    switched_result = attend_unit_results(
        query_sum.astype(jnp.bfloat16),
        key_sum.astype(jnp.bfloat16),
        value_sum.astype(jnp.bfloat16),
        gate_sum.astype(jnp.bfloat16),
        decay_sum + forgetting_shift,
        spike_forget_logarithm,
        attend_unit_scale,
    )
    mixer_partial = jnp.dot(
        switched_result,
        lax.all_gather(attend_result_matrix, "fs", axis=1, tiled=True),
        preferred_element_type=jnp.float32,
    )
    mix = lax.psum_scatter(
        mixer_partial.astype(jnp.bfloat16), "tp", scatter_dimension=1, tiled=True
    )
    middle = (
        incoming_features.astype(jnp.float32) + lax.optimization_barrier(mix).astype(jnp.float32)
    ).astype(jnp.bfloat16)
    whole_mid = lax.all_gather(middle, "tp", axis=1, tiled=True)
    normed_mid = row_norm(whole_mid, perceptron_scale)
    pieces = (
        lax.all_gather(content_expand_matrix, "fs", axis=0, tiled=True),
        lax.all_gather(switch_expand_matrix, "fs", axis=0, tiled=True),
    )
    columns = normed_mid
    value_total = jnp.dot(columns, pieces[0], preferred_element_type=jnp.float32)
    gate_total = jnp.dot(columns, pieces[1], preferred_element_type=jnp.float32)
    conv_value = causal_conv(value_total.astype(jnp.bfloat16), content_kernel)
    conv_gated = causal_conv(gate_total.astype(jnp.bfloat16), switch_kernel)
    hidden = (conv_value * jax.nn.gelu(conv_gated, approximate=True)).astype(jnp.bfloat16)
    down_partial = jnp.dot(
        hidden,
        lax.all_gather(contract_matrix, "fs", axis=1, tiled=True),
        preferred_element_type=jnp.float32,
    )
    ffn = lax.psum_scatter(down_partial.astype(jnp.bfloat16), "tp", scatter_dimension=1, tiled=True)
    return (middle.astype(jnp.float32) + lax.optimization_barrier(ffn).astype(jnp.float32)).astype(
        jnp.bfloat16
    )


def solution(mesh):
    placed = (
        P(("rep", "fs"), "tp"),
        P(),
        P("fs", "tp"),
        P("fs", "tp"),
        P("fs", "tp"),
        P("fs", "tp"),
        P("fs", "tp"),
        P("tp"),
        P(("rep", "fs"), "tp"),
        P("tp"),
        P("tp", "fs"),
        P(),
        P("fs", "tp"),
        P("fs", "tp"),
        P(None, "tp"),
        P(None, "tp"),
        P("tp", "fs"),
    )
    return jax.shard_map(
        shards, mesh=mesh, in_specs=placed, out_specs=P(("rep", "fs"), "tp"), check_vma=False
    )
```

profile of v0, /device:TPU:0, one launch (start us, length us, event | category | flops | bytes accessed | tf_op | source)
XLA Modules:
  0.0 697.6 jit_solution(7244822778492802372)
XLA Ops:
  10.6 2.7 all_gather.33
  13.5 39.0 %all-gather.10.cloned.1.call-done = bf16[2048,256]{1,0:T(8,128)(2,1)} async-done(((bf16[256,256]{1,0:T(8,128)(2,1)}), bf16[2048,256]{1,0:T(8,128)(2,1)}) %all-gather.10.cloned.1.call-update) | async-done | bytes 1048592 | tf_op jit(solution)/shard_map/all_gather | solution.py:133
  52.5 1.7 fusion.65
  55.4 38.2 %all-gather.12.cloned.1.call-done = bf16[2048,256]{1,0:T(8,128)(2,1)} async-done(((bf16[256,256]{1,0:T(8,128)(2,1)}), bf16[2048,256]{1,0:T(8,128)(2,1)}) %all-gather.12.cloned.1.call-update) | async-done | bytes 1048592 | tf_op jit(solution)/shard_map/all_gather | solution.py:131
  93.7 1.7 fusion.47
  95.5 39.3 %all-gather.16.cloned.1.call-done = bf16[2048,256]{1,0:T(8,128)(2,1)} async-done(((bf16[256,256]{1,0:T(8,128)(2,1)}), bf16[2048,256]{1,0:T(8,128)(2,1)}) %all-gather.16.cloned.1.call-update) | async-done | bytes 1048592 | tf_op jit(solution)/shard_map/all_gather | solution.py:130
  134.8 1.7 fusion.46
  136.7 47.9 %all-gather.14.cloned.1.call-done = bf16[2048,512]{1,0:T(8,128)(2,1)} async-done(((bf16[256,512]{1,0:T(8,128)(2,1)}), bf16[2048,512]{1,0:T(8,128)(2,1)}) %all-gather.14.cloned.1.call-update) | async-done | bytes 2097168 | tf_op jit(solution)/shard_map/all_gather | solution.py:132
  184.6 2.2 fusion.43
  187.9 73.7 %while.13 = (s32[]{:T(128)}, f32[8,32,64]{2,1,0:T(8,128)S(1)}, f32[3,64,8,64]{1,3,2,0:T(8,128)}, f32[3,64,8,32]{3,2,1,0:T(8,128)}, f32[3,64,8,32]{3,2,1,0:T(8,12...) while((s32[]{:T(128)}, f32[8,32,64]{2,1,0:T(8,128)S(1)}, ...), condition=%wide.region_3.4_spmd.clone, body=%wide.region_1.3_spmd.clone.sunk | while | flops 56725504 | bytes 20003956 | solution.py:52
  189.1 4.7 select_exponential_fusion.2
  193.8 9.5 %copy.122 = f32[64,64,8,32]{0,1,3,2:T(8,128)} copy(f32[64,64,8,32]{1,3,2,0:T(8,128)} %select_exponential_fusion.2) | data formatting | bytes 8388608 | tf_op jit(solution)/shard_map/while
  203.6 5.3 fusion.108
  213.7 4.6 select_exponential_fusion.2
  218.3 9.5 %copy.122 = f32[64,64,8,32]{0,1,3,2:T(8,128)} copy(f32[64,64,8,32]{1,3,2,0:T(8,128)} %select_exponential_fusion.2) | data formatting | bytes 8388608 | tf_op jit(solution)/shard_map/while
  228.1 5.2 fusion.108
  238.2 4.7 select_exponential_fusion.2
  242.9 9.6 %copy.122 = f32[64,64,8,32]{0,1,3,2:T(8,128)} copy(f32[64,64,8,32]{1,3,2,0:T(8,128)} %select_exponential_fusion.2) | data formatting | bytes 8388608 | tf_op jit(solution)/shard_map/while
  252.8 5.3 fusion.108
  261.7 1.5 copy.86
  263.9 21.1 %all-gather.20.cloned.1.call-done = bf16[512,2048]{1,0:T(8,128)(2,1)} async-done(((bf16[512,256]{1,0:T(8,128)(2,1)}), bf16[512,2048]{1,0:T(8,128)(2,1)}) %all-gather.20.cloned.1.call-update) | async-done | bytes 2097168 | tf_op jit(solution)/shard_map/all_gather | solution.py:151
  285.0 4.4 convolution_convert_fusion.3
  291.7 4.3 reduce-scatter.3.cloned.1.call-done
  297.1 2.5 all_gather.40
  299.9 123.8 %all-gather.24.cloned.1.call-done = bf16[2048,2048]{1,0:T(8,128)(2,1)} async-done(((bf16[256,2048]{1,0:T(8,128)(2,1)}), bf16[2048,2048]{1,0:T(8,128)(2,1)}) %all-gather.24.cloned.1.call-update) | async-done | bytes 8388624 | tf_op jit(solution)/shard_map/all_gather | solution.py:164
  423.7 5.2 fusion.17
  428.9 119.6 %all-gather.22.cloned.1.call-done = bf16[2048,2048]{1,0:T(8,128)(2,1)} async-done(((bf16[256,2048]{1,0:T(8,128)(2,1)}), bf16[2048,2048]{1,0:T(8,128)(2,1)}) %all-gather.22.cloned.1.call-update) | async-done | bytes 8388624 | tf_op jit(solution)/shard_map/all_gather | solution.py:163
  548.5 6.4 fusion.18
  554.9 118.6 %all-gather.26.cloned.1.call-done = bf16[2048,2048]{1,0:T(8,128)(2,1)} async-done(((bf16[2048,256]{1,0:T(8,128)(2,1)}), bf16[2048,2048]{1,0:T(8,128)(2,1)}) %all-gather.26.cloned.1.call-update) | async-done | bytes 8388624 | tf_op jit(solution)/shard_map/all_gather | solution.py:174
  673.6 9.0 %convolution_convert_fusion = bf16[192,2048]{1,0:T(8,128)(2,1)} fusion(bf16[2048,2048]{1,0:T(8,128)(2,1)} %all-gather.26.cloned.1.call-done, f32[192,2048]{1,0:T(8,128)} %fusion.18, f32[192,2048]{1,0:T(8,128)S(1)} %fusion.17, f32[2048]{0:T(1024)S(1)} %bitcast.92, f32[2048]{0:T(1024)S(1)} %bitcast.91, f32[2048]{0:T(1024)S(1)} %bitcast.90, ...), kind=kOutput, calls=%fused_computation.29 | convolution fusion | flops 1618870272 | bytes 12369920 | tf_op jit(solution)/shard_map/dot_general | solution.py:172
  682.7 6.5 reduce-scatter.5.cloned.1.call-done
  689.1 1.9 add_convert_fusion
  (107 shorter events, 26.2 us)
Async XLA Ops:
  6.5 7.0 %copy-start.6 = (bf16[2048]{0:T(1024)(128)(2,1)S(1)}, bf16[2048]{0:T(1024)(128)(2,1)}, u32[]{:S(2)}) copy-start(bf16[2048]{0:T(1024)(128)(2,1)} %param.20) | copy-start | bytes 12292
  6.5 7.0 %copy-start.8 = (bf16[512]{0:T(512)(128)(2,1)S(1)}, bf16[512]{0:T(512)(128)(2,1)}, u32[]{:S(2)}) copy-start(bf16[512]{0:T(512)(128)(2,1)} %param.28) | copy-start | bytes 3076
  6.5 46.0 %copy-start.9 = (f32[192,256]{1,0:T(8,128)S(1)}, f32[192,256]{1,0:T(8,128)}, u32[]{:S(2)}) copy-start(f32[192,256]{1,0:T(8,128)} %param.27) | copy-start | bytes 589828
  6.5 46.0 %copy-start.10 = (f32[256]{0:T(256)S(1)}, f32[256]{0:T(256)}, u32[]{:S(2)}) copy-start(f32[256]{0:T(256)} %param.26) | copy-start | bytes 3076
  6.5 46.0 %all-gather.10.cloned.1.call-start = ((), (), s32[]{:S(2)}) async-start(), calls=%async_computation.2 | async-start | bytes 1179648 | tf_op jit(solution)/shard_map/all_gather | solution.py:133
  7.3 86.4 %all-gather.12.cloned.1.call-start = ((), (), s32[]{:S(2)}) async-start(), calls=%async_computation.3 | async-start | bytes 1179648 | tf_op jit(solution)/shard_map/all_gather | solution.py:131
  8.0 126.8 %all-gather.16.cloned.1.call-start = ((), (), s32[]{:S(2)}) async-start(), calls=%async_computation.5 | async-start | bytes 1179648 | tf_op jit(solution)/shard_map/all_gather | solution.py:130
  8.8 175.9 %all-gather.14.cloned.1.call-start = ((), (), s32[]{:S(2)}) async-start(), calls=%async_computation.4 | async-start | bytes 2359296 | tf_op jit(solution)/shard_map/all_gather | solution.py:132
  9.3 254.6 %all-gather.18.cloned.1.call-start = ((), (), s32[]{:S(2)}) async-start(), calls=%async_computation.6 | async-start | bytes 2359296 | tf_op jit(solution)/shard_map/all_gather | solution.py:134
  9.9 275.1 %all-gather.20.cloned.1.call-start = ((), (), s32[]{:S(2)}) async-start(), calls=%async_computation.7 | async-start | bytes 2359296 | tf_op jit(solution)/shard_map/all_gather | solution.py:151
  10.5 285.5 %reduce-scatter.3.cloned.1.call-start = ((), (), s32[]{:S(2)}) async-start(), calls=%async_computation.8 | async-start | bytes 1179648 | tf_op jit(solution)/shard_map/reduce_scatter | solution.py:154
  13.3 171.4 %copy-start = (bf16[192,2048]{1,0:T(8,128)(2,1)}, bf16[192,2048]{1,0:T(8,128)(2,1)S(1)}, u32[]{:S(2)}) copy-start(bf16[192,2048]{1,0:T(8,128)(2,1)S(1)} %all_gather.33) | copy-start | bytes 2359300
  261.7 1.8 copy-start.2
  263.2 21.8 %copy-start.1 = (bf16[192,2048]{1,0:T(8,128)(2,1)S(1)}, bf16[192,2048]{1,0:T(8,128)(2,1)}, u32[]{:S(2)}) copy-start(bf16[192,2048]{1,0:T(8,128)(2,1)} %copy-done) | copy-start | bytes 2359300
  289.4 2.2 copy-start.7
  289.4 2.2 copy-start.4
  289.5 2.2 copy-start.5
  289.5 6.5 copy-start.3
  289.5 134.2 %all-gather.24.cloned.1.call-start = ((), (), s32[]{:S(2)}) async-start(), calls=%async_computation.10 | async-start | bytes 9437184 | tf_op jit(solution)/shard_map/all_gather | solution.py:164
  290.2 258.3 %all-gather.22.cloned.1.call-start = ((), (), s32[]{:S(2)}) async-start(), calls=%async_computation.9 | async-start | bytes 9437184 | tf_op jit(solution)/shard_map/all_gather | solution.py:163
  291.0 382.6 %all-gather.26.cloned.1.call-start = ((), (), s32[]{:S(2)}) async-start(), calls=%async_computation.11 | async-start | bytes 9437184 | tf_op jit(solution)/shard_map/all_gather | solution.py:174
  291.5 397.6 %reduce-scatter.5.cloned.1.call-start = ((), (), s32[]{:S(2)}) async-start(), calls=%async_computation.12 | async-start | bytes 1179648 | tf_op jit(solution)/shard_map/reduce_scatter | solution.py:177
Sparse Core Ops, SparseCore 0:
  9.5 42.9 all-gather.9
  54.6 38.9 all-gather.11
  95.8 38.9 all-gather.15
  136.8 47.7 all-gather.13
  186.6 47.6 all-gather.17
  236.1 48.8 all-gather.19
  289.5 6.3 reduce-scatter.2
  298.1 125.5 all-gather.23
  425.8 122.6 all-gather.21
  550.4 123.1 all-gather.25
  682.8 6.3 reduce-scatter.4
where the time goes:
time: 699 us; the launch traced here: 698 us
  waiting for transfers between devices  564 us (81%)
  matrix products  39.9 us (6%)
  local copies, waits for them, and re-layouts  37.6 us (5%)
  other arithmetic  36.7 us (5%)
  between operations  13.5 us (2%)
    all_gather x1, waiting for transfers between devices, shards(): lax.all_gather(switch_expand_matrix, 'fs', axis=0, tiled=True)  124 us
    all_gather x1, waiting for transfers between devices, shards(): lax.all_gather(content_expand_matrix, 'fs', axis=0, tiled=True)  120 us
    all_gather x1, waiting for transfers between devices, shards(): lax.all_gather(contract_matrix, 'fs', axis=1, tiled=True)  119 us
    all_gather x1, waiting for transfers between devices, shards(): lax.all_gather(content_matrix, 'fs', axis=0, tiled=True)  47.9 us
    all_gather x1, waiting for transfers between devices, shards(): lax.all_gather(probe_matrix, 'fs', axis=0, tiled=True)  39.3 us
    all_gather x1, waiting for transfers between devices, shards(): lax.all_gather(forgetting_matrix, 'fs', axis=0, tiled=True)  39 us
    all_gather x1, waiting for transfers between devices, shards(): lax.all_gather(lookup_matrix, 'fs', axis=0, tiled=True)  38.2 us
    while x3, local copies, waits for them, and re-layouts  28.6 us
  transfers between devices with their start and end apart: 11, of which 10 were waited for; matrix products, arithmetic and copies ran while one was open for 14% of the time, Pallas kernels for 0%

commit v1 on v0

--- a/solution.py
+++ b/solution.py
@@ -124,6 +124,11 @@
     switch_kernel,
     contract_matrix,
 ):
+
+    def handle_the_copies(tile_in):
+        arr_out = jnp.concatenate(lax.all_gather(tile_in, "fs"), 1)
+        return arr_out
+
     whole_in = lax.all_gather(incoming_features, "tp", axis=1, tiled=True)
     normed = row_norm(whole_in, attend_prenormal_scale)
     pieces = (
@@ -170,9 +175,7 @@
     conv_gated = causal_conv(gate_total.astype(jnp.bfloat16), switch_kernel)
     hidden = (conv_value * jax.nn.gelu(conv_gated, approximate=True)).astype(jnp.bfloat16)
     down_partial = jnp.dot(
-        hidden,
-        lax.all_gather(contract_matrix, "fs", axis=1, tiled=True),
-        preferred_element_type=jnp.float32,
+        hidden, handle_the_copies(contract_matrix), preferred_element_type=jnp.float32
     )
     ffn = lax.psum_scatter(down_partial.astype(jnp.bfloat16), "tp", scatter_dimension=1, tiled=True)
     return (middle.astype(jnp.float32) + lax.optimization_barrier(ffn).astype(jnp.float32)).astype(

time: 699 us -> 700 us (level)
  local copies, waits for them, and re-layouts: 37.6 us -> 49.7 us
    reshape x0 -> x1, local copies, waits for them, and re-layouts: none -> 11.7 us  [handle_the_copies(): arr_out = jnp.concatenate(lax.all_gather(tile_in, 'fs'), 1)]
    all_gather x1, waiting for transfers between devices: 124 us -> 113 us  [shards(): lax.all_gather(switch_expand_matrix, 'fs', axis=0, tiled=True)]
  transfers between devices with their start and end apart: 11 -> 11, of which waited for: 10 -> 10; matrix products, arithmetic and copies ran while one was open for 14% -> 15% of each run, Pallas kernels for 0% -> 0%
where the time goes in v1:
time: 700 us; the launch traced here: 699 us
  waiting for transfers between devices  558 us (80%)
  local copies, waits for them, and re-layouts  49.7 us (7%)
  other arithmetic  36.6 us (5%)
  matrix products  34.5 us (5%)
  between operations  13.5 us (2%)
    all_gather x1, waiting for transfers between devices, handle_the_copies(): arr_out = jnp.concatenate(lax.all_gather(tile_in, 'fs'), 1)  124 us
    all_gather x1, waiting for transfers between devices, shards(): lax.all_gather(content_expand_matrix, 'fs', axis=0, tiled=True)  119 us
    all_gather x1, waiting for transfers between devices, shards(): lax.all_gather(switch_expand_matrix, 'fs', axis=0, tiled=True)  113 us
    all_gather x1, waiting for transfers between devices, shards(): lax.all_gather(content_matrix, 'fs', axis=0, tiled=True)  47.9 us
    all_gather x1, waiting for transfers between devices, shards(): lax.all_gather(probe_matrix, 'fs', axis=0, tiled=True)  39.3 us
    all_gather x1, waiting for transfers between devices, shards(): lax.all_gather(forgetting_matrix, 'fs', axis=0, tiled=True)  39 us
    all_gather x1, waiting for transfers between devices, shards(): lax.all_gather(lookup_matrix, 'fs', axis=0, tiled=True)  38.2 us
    while x3, local copies, waits for them, and re-layouts  28.6 us
  transfers between devices with their start and end apart: 11, of which 10 were waited for; matrix products, arithmetic and copies ran while one was open for 15% of the time, Pallas kernels for 0%

profile of v1, /device:TPU:0, one launch (start us, length us, event | category | flops | bytes accessed | tf_op | source)
XLA Modules:
  0.0 698.6 jit_solution(8128798606076120107)
XLA Ops:
  10.6 2.7 all_gather.36
  13.5 39.0 %all-gather.11.cloned.1.call-done = bf16[2048,256]{1,0:T(8,128)(2,1)} async-done(((bf16[256,256]{1,0:T(8,128)(2,1)}), bf16[2048,256]{1,0:T(8,128)(2,1)}) %all-gather.11.cloned.1.call-update) | async-done | bytes 1048592 | tf_op jit(solution)/shard_map/all_gather | solution.py:138
  52.5 1.7 fusion.65
  55.4 38.2 %all-gather.13.cloned.1.call-done = bf16[2048,256]{1,0:T(8,128)(2,1)} async-done(((bf16[256,256]{1,0:T(8,128)(2,1)}), bf16[2048,256]{1,0:T(8,128)(2,1)}) %all-gather.13.cloned.1.call-update) | async-done | bytes 1048592 | tf_op jit(solution)/shard_map/all_gather | solution.py:136
  93.7 1.7 fusion.47
  95.5 39.3 %all-gather.17.cloned.1.call-done = bf16[2048,256]{1,0:T(8,128)(2,1)} async-done(((bf16[256,256]{1,0:T(8,128)(2,1)}), bf16[2048,256]{1,0:T(8,128)(2,1)}) %all-gather.17.cloned.1.call-update) | async-done | bytes 1048592 | tf_op jit(solution)/shard_map/all_gather | solution.py:135
  134.8 1.7 fusion.46
  136.7 47.9 %all-gather.15.cloned.1.call-done = bf16[2048,512]{1,0:T(8,128)(2,1)} async-done(((bf16[256,512]{1,0:T(8,128)(2,1)}), bf16[2048,512]{1,0:T(8,128)(2,1)}) %all-gather.15.cloned.1.call-update) | async-done | bytes 2097168 | tf_op jit(solution)/shard_map/all_gather | solution.py:137
  184.6 2.2 fusion.43
  187.9 73.6 %while.13 = (s32[]{:T(128)}, f32[8,32,64]{2,1,0:T(8,128)S(1)}, f32[3,64,8,64]{1,3,2,0:T(8,128)}, f32[3,64,8,32]{3,2,1,0:T(8,128)}, f32[3,64,8,32]{3,2,1,0:T(8,12...) while((s32[]{:T(128)}, f32[8,32,64]{2,1,0:T(8,128)S(1)}, ...), condition=%wide.region_3.4_spmd.clone, body=%wide.region_1.3_spmd.clone.sunk | while | flops 56725504 | bytes 20003956 | solution.py:52
  189.1 4.6 select_exponential_fusion.2
  193.7 9.5 %copy.125 = f32[64,64,8,32]{0,1,3,2:T(8,128)} copy(f32[64,64,8,32]{1,3,2,0:T(8,128)} %select_exponential_fusion.2) | data formatting | bytes 8388608 | tf_op jit(solution)/shard_map/while
  203.5 5.3 fusion.108
  213.6 4.6 select_exponential_fusion.2
  218.2 9.5 %copy.125 = f32[64,64,8,32]{0,1,3,2:T(8,128)} copy(f32[64,64,8,32]{1,3,2,0:T(8,128)} %select_exponential_fusion.2) | data formatting | bytes 8388608 | tf_op jit(solution)/shard_map/while
  228.0 5.2 fusion.108
  238.1 4.6 select_exponential_fusion.2
  242.7 9.6 %copy.125 = f32[64,64,8,32]{0,1,3,2:T(8,128)} copy(f32[64,64,8,32]{1,3,2,0:T(8,128)} %select_exponential_fusion.2) | data formatting | bytes 8388608 | tf_op jit(solution)/shard_map/while
  252.6 5.3 fusion.108
  263.7 21.3 %all-gather.21.cloned.1.call-done = bf16[512,2048]{1,0:T(8,128)(2,1)} async-done(((bf16[512,256]{1,0:T(8,128)(2,1)}), bf16[512,2048]{1,0:T(8,128)(2,1)}) %all-gather.21.cloned.1.call-update) | async-done | bytes 2097168 | tf_op jit(solution)/shard_map/all_gather | solution.py:156
  285.1 4.4 convolution_convert_fusion.3
  291.7 4.2 reduce-scatter.3.cloned.1.call-done
  297.1 2.5 all_gather.43
  299.9 123.8 %all-gather.27.cloned.1.call-done = bf16[16384,256]{1,0:T(8,128)(2,1)} async-done(((bf16[2048,256]{1,0:T(8,128)(2,1)}), bf16[16384,256]{1,0:T(8,128)(2,1)}) %all-gather.27.cloned.1.call-update) | async-done | bytes 8388624 | tf_op jit(solution)/shard_map/all_gather | solution.py:129
  423.7 11.7 %copy.91 = bf16[2048,8,256]{0,2,1:T(8,128)(2,1)} copy(bf16[2048,8,256]{2,0,1:T(8,128)(2,1)} %bitcast.90) | data formatting | bytes 16777216 | tf_op jit(solution)/shard_map/reshape | solution.py:129
  435.4 113.1 %all-gather.25.cloned.1.call-done = bf16[2048,2048]{1,0:T(8,128)(2,1)} async-done(((bf16[256,2048]{1,0:T(8,128)(2,1)}), bf16[2048,2048]{1,0:T(8,128)(2,1)}) %all-gather.25.cloned.1.call-update) | async-done | bytes 8388624 | tf_op jit(solution)/shard_map/all_gather | solution.py:169
  548.5 5.2 fusion.17
  553.8 119.4 %all-gather.23.cloned.1.call-done = bf16[2048,2048]{1,0:T(8,128)(2,1)} async-done(((bf16[256,2048]{1,0:T(8,128)(2,1)}), bf16[2048,2048]{1,0:T(8,128)(2,1)}) %all-gather.23.cloned.1.call-update) | async-done | bytes 8388624 | tf_op jit(solution)/shard_map/all_gather | solution.py:168
  673.2 5.4 fusion.18
  679.0 4.7 convolution_convert_fusion
  683.7 6.5 reduce-scatter.5.cloned.1.call-done
  690.2 1.9 add_convert_fusion
  (110 shorter events, 28.1 us)
Async XLA Ops:
  6.5 7.0 copy-start.7
  6.5 7.0 %copy-start.9 = (bf16[512]{0:T(512)(128)(2,1)S(1)}, bf16[512]{0:T(512)(128)(2,1)}, u32[]{:S(2)}) copy-start(bf16[512]{0:T(512)(128)(2,1)} %param.28) | copy-start | bytes 3076
  6.5 46.0 %copy-start.10 = (f32[192,256]{1,0:T(8,128)S(1)}, f32[192,256]{1,0:T(8,128)}, u32[]{:S(2)}) copy-start(f32[192,256]{1,0:T(8,128)} %param.27) | copy-start | bytes 589828
  6.5 46.0 %copy-start.11 = (f32[256]{0:T(256)S(1)}, f32[256]{0:T(256)}, u32[]{:S(2)}) copy-start(f32[256]{0:T(256)} %param.26) | copy-start | bytes 3076
  6.5 46.0 %all-gather.11.cloned.1.call-start = ((), (), s32[]{:S(2)}) async-start(), calls=%async_computation.2 | async-start | bytes 1179648 | tf_op jit(solution)/shard_map/all_gather | solution.py:138
  7.3 86.4 %all-gather.13.cloned.1.call-start = ((), (), s32[]{:S(2)}) async-start(), calls=%async_computation.3 | async-start | bytes 1179648 | tf_op jit(solution)/shard_map/all_gather | solution.py:136
  8.0 126.8 %all-gather.17.cloned.1.call-start = ((), (), s32[]{:S(2)}) async-start(), calls=%async_computation.5 | async-start | bytes 1179648 | tf_op jit(solution)/shard_map/all_gather | solution.py:135
  8.8 175.9 %all-gather.15.cloned.1.call-start = ((), (), s32[]{:S(2)}) async-start(), calls=%async_computation.4 | async-start | bytes 2359296 | tf_op jit(solution)/shard_map/all_gather | solution.py:137
  9.3 254.4 %all-gather.19.cloned.1.call-start = ((), (), s32[]{:S(2)}) async-start(), calls=%async_computation.6 | async-start | bytes 2359296 | tf_op jit(solution)/shard_map/all_gather | solution.py:139
  9.9 275.1 %all-gather.21.cloned.1.call-start = ((), (), s32[]{:S(2)}) async-start(), calls=%async_computation.7 | async-start | bytes 2359296 | tf_op jit(solution)/shard_map/all_gather | solution.py:156
  10.5 285.4 %reduce-scatter.3.cloned.1.call-start = ((), (), s32[]{:S(2)}) async-start(), calls=%async_computation.8 | async-start | bytes 1179648 | tf_op jit(solution)/shard_map/reduce_scatter | solution.py:159
  13.3 171.4 %copy-start.1 = (bf16[192,2048]{1,0:T(8,128)(2,1)}, bf16[192,2048]{1,0:T(8,128)(2,1)S(1)}, u32[]{:S(2)}) copy-start(bf16[192,2048]{1,0:T(8,128)(2,1)S(1)} %all_gather.36) | copy-start | bytes 2359300
  261.5 1.8 copy-start.3
  263.0 22.0 %copy-start.2 = (bf16[192,2048]{1,0:T(8,128)(2,1)S(1)}, bf16[192,2048]{1,0:T(8,128)(2,1)}, u32[]{:S(2)}) copy-start(bf16[192,2048]{1,0:T(8,128)(2,1)} %copy-done.1) | copy-start | bytes 2359300
  289.5 2.2 copy-start.8
  289.5 2.2 copy-start.5
  289.5 2.2 copy-start.6
  289.5 6.4 copy-start.4
  289.5 134.2 %all-gather.27.cloned.1.call-start = ((), (), s32[]{:S(2)}) async-start(), calls=%async_computation.12 | async-start | bytes 9437184 | tf_op jit(solution)/shard_map/all_gather | solution.py:129
  290.3 258.3 %all-gather.25.cloned.1.call-start = ((), (), s32[]{:S(2)}) async-start(), calls=%async_computation.10 | async-start | bytes 9437184 | tf_op jit(solution)/shard_map/all_gather | solution.py:169
  291.0 382.2 %all-gather.23.cloned.1.call-start = ((), (), s32[]{:S(2)}) async-start(), calls=%async_computation.9 | async-start | bytes 9437184 | tf_op jit(solution)/shard_map/all_gather | solution.py:168
  291.6 398.6 %reduce-scatter.5.cloned.1.call-start = ((), (), s32[]{:S(2)}) async-start(), calls=%async_computation.11 | async-start | bytes 1179648 | tf_op jit(solution)/shard_map/reduce_scatter | solution.py:180
  673.2 5.8 copy-start
Sparse Core Ops, SparseCore 0:
  9.5 42.9 all-gather.10
  54.6 38.9 all-gather.12
  95.8 38.9 all-gather.16
  136.8 47.7 all-gather.14
  186.6 47.6 all-gather.18
  236.1 48.8 all-gather.20
  289.6 6.2 reduce-scatter.2
  298.1 125.6 all-gather.26
  425.8 122.6 all-gather.24
  550.5 122.6 all-gather.22
  683.8 6.3 reduce-scatter.4
